TPU v7x, 32 devices: a whole 2x2x4 slice. The times are simulated.
32 devices in a mesh: ep: 8 (over z, x), tp: 4 (over y, core).
Axes of the slice: x: 2, y: 2, z: 4, core: 2. Of those that a mesh axis runs over, the one named last changes fastest.
Arguments:
- tokens: bfloat16 [128, 1024], P('ep'), may hold values from -6 to 6
- memory: float32 [128, 4, 128, 256], P('ep', 'tp'), may hold values from -6 to 6
- log_scale: float32 [128, 4], P('ep', 'tp'), may hold values from -1 to 130
- mix_gain_in: float32 [1024], replicated, may hold values from 0.1 to 1.9
- w_query: bfloat16 [1024, 512], P(None, 'tp'), may hold values from -0.1875 to 0.1875
- w_key: bfloat16 [1024, 512], P(None, 'tp'), may hold values from -0.1875 to 0.1875
- w_value: bfloat16 [1024, 1024], P(None, 'tp'), may hold values from -0.1875 to 0.1875
- w_igate: bfloat16 [1024, 4], P(None, 'tp'), may hold values from -0.1875 to 0.1875
- w_fgate: bfloat16 [1024, 4], P(None, 'tp'), may hold values from -0.1875 to 0.1875
- igate_bias: float32 [4], P('tp'), may hold values from -1 to 1
- fgate_bias: float32 [4], P('tp'), may hold values from 0 to 4
- head_gain: float32 [1024], P('tp'), may hold values from 0.1 to 1.9
- w_output: bfloat16 [1024, 1024], P('tp'), may hold values from -0.1875 to 0.1875
- mix_gain_out: float32 [1024], replicated, may hold values from 0.1 to 1.9
- ffn_gain_in: float32 [1024], replicated, may hold values from 0.1 to 1.9
- routes: int32 [128, 6], P('ep'), may hold values from 0 to 7, all different within a row; in each aligned block of 16 rows (0 to 15, 16 to 31, ...) at most 16 rows name the same one
- route_weights: float32 [128, 6], P('ep'), may hold values from 0.1 to 1
- expert_gate: bfloat16 [8, 1024, 1024], P('ep', None, 'tp'), may hold values from -0.1875 to 0.1875
- expert_up: bfloat16 [8, 1024, 1024], P('ep', None, 'tp'), may hold values from -0.1875 to 0.1875
- expert_down: bfloat16 [8, 1024, 1024], P('ep', 'tp'), may hold values from -0.9375 to 0.9375
- ffn_gain_out: float32 [1024], P('tp'), may hold values from 0.1 to 1.9
Outputs:
- output: bfloat16 [128, 1024], P('ep', 'tp')
Inputs may be any that keep to these rules, and one draw needn't show every extreme that they name: `routes`: among the 16 tokens of one index of ep no expert is named by more than 16 tokens, and in every draw some expert is named by exactly 16 of them.
All inputs are finite; a program needn't handle non-finite values.
Results may differ from a plain program's by a relative error of at most 0.02.
Values may be sent and summed in bfloat16 or wider, within the bound.
A program may use at most 64 MiB of HBM per device.

v0:
```python
import jax
import jax.numpy as jnp
from jax import lax
from jax.sharding import PartitionSpec as P

EPS = 1e-06


def rms_scale(values):
    return lax.rsqrt(jnp.mean(values * values, axis=-1, keepdims=True) + EPS)


def per_device(
    tokens,
    memory,
    log_scale,
    mix_gain_in,
    w_query,
    w_key,
    w_value,
    w_igate,
    w_fgate,
    igate_bias,
    fgate_bias,
    head_gain,
    w_output,
    mix_gain_out,
    ffn_gain_in,
    routes,
    route_weights,
    expert_gate,
    expert_up,
    expert_down,
    ffn_gain_out,
):
    f32 = jnp.float32
    bf16 = jnp.bfloat16
    seqs, width = tokens.shape
    heads = log_scale.shape[1]
    key_dim = memory.shape[2]
    value_dim = memory.shape[3]
    xf = tokens.astype(f32)
    normed = (xf * rms_scale(xf) * mix_gain_in).astype(bf16)
    query = jnp.dot(normed, w_query, preferred_element_type=f32).reshape(
        seqs, heads, key_dim
    ) * key_dim ** (-0.5)
    keys = jnp.dot(normed, w_key, preferred_element_type=f32).reshape(seqs, heads, key_dim)
    values = jnp.dot(normed, w_value, preferred_element_type=f32).reshape(seqs, heads, value_dim)
    in_pre = jnp.dot(normed, w_igate, preferred_element_type=f32) + igate_bias
    forget_log = jax.nn.log_sigmoid(
        jnp.dot(normed, w_fgate, preferred_element_type=f32) + fgate_bias
    )
    carried = forget_log + log_scale
    new_max = jnp.maximum(carried, in_pre)
    carry_weight = jnp.exp(carried - new_max)
    fresh_weight = jnp.exp(in_pre - new_max)
    recall = jnp.einsum("shk,shkv->shv", query, memory, precision=lax.Precision.HIGHEST)
    match = jnp.sum(query * keys, axis=-1)
    read = carry_weight[..., None] * recall + (fresh_weight * match)[..., None] * values
    headout = (
        (read * rms_scale(read) * head_gain.reshape(heads, value_dim))
        .astype(bf16)
        .reshape(seqs, heads * value_dim)
    )
    partial_value = jnp.dot(headout, w_output, preferred_element_type=f32)
    mixed = lax.psum(partial_value.astype(jnp.bfloat16), "tp").astype(jnp.float32)
    resid = (xf + mixed * rms_scale(mixed) * mix_gain_out).astype(bf16)
    rf = resid.astype(f32)
    ffn_in = (rf * rms_scale(rf) * ffn_gain_in).astype(bf16)
    lanes = lax.axis_size("tp")
    quarter = width // lanes
    own = lax.axis_index("tp") * quarter
    local_experts = expert_gate.shape[0]
    experts_all = local_experts * lax.axis_size("ep")
    top = routes.shape[1]
    cap = min(seqs, max(2, 3 * seqs * top // (2 * experts_all)))
    flat = routes.reshape(-1)
    hits = (flat[:, None] == jnp.arange(experts_all, dtype=jnp.int32)[None, :]).astype(jnp.int32)
    earlier = jnp.cumsum(hits, axis=0) - hits
    slot = jnp.sum(earlier * hits, axis=1)
    place = (flat * cap + slot).reshape(seqs, top)
    picker = jnp.any(
        jnp.arange(experts_all * cap, dtype=jnp.int32)[:, None, None] == place[None, :, :], axis=2
    ).astype(bf16)
    outbound = (
        jnp.dot(picker, ffn_in, preferred_element_type=f32)
        .astype(bf16)
        .reshape(experts_all, cap, width)
    )
    arrived = lax.all_to_all(outbound, "ep", split_axis=0, concat_axis=0, tiled=True)
    items = arrived.shape[1]
    rows = arrived.reshape(-1, local_experts, items, width)
    gate = jnp.einsum("secd,edf->secf", rows, expert_gate, preferred_element_type=f32)
    up = jnp.einsum("secd,edf->secf", rows, expert_up, preferred_element_type=f32)
    act = (jax.nn.silu(gate) * up).astype(bf16)
    part = jnp.einsum("secf,efd->secd", act, expert_down, preferred_element_type=f32).reshape(
        -1, items, width
    )
    summed = lax.psum_scatter(
        part.astype(jnp.bfloat16), "tp", scatter_dimension=2, tiled=True
    ).astype(jnp.float32)
    done = summed.astype(bf16)
    returned = lax.all_to_all(done, "ep", split_axis=0, concat_axis=0, tiled=True)
    columns = returned.shape[2]
    chosen = jnp.take(returned.reshape(-1, columns), place.reshape(-1), axis=0).reshape(
        seqs, top, columns
    )
    routed = jnp.sum(route_weights[:, :, None] * chosen.astype(f32), axis=1)
    resid_part = lax.dynamic_slice_in_dim(rf, own, quarter, 1)
    total = lax.psum(jnp.sum(routed * routed, axis=1), "tp")
    scaled = routed * lax.rsqrt(total / width + EPS)[:, None]
    return (resid_part + scaled * ffn_gain_out).astype(bf16)


def solution(mesh):
    return jax.shard_map(
        per_device,
        mesh=mesh,
        in_specs=(
            P("ep", None),
            P("ep", "tp", None, None),
            P("ep", "tp"),
            P(),
            P(None, "tp"),
            P(None, "tp"),
            P(None, "tp"),
            P(None, "tp"),
            P(None, "tp"),
            P("tp"),
            P("tp"),
            P("tp"),
            P("tp", None),
            P(),
            P(),
            P("ep", None),
            P("ep", None),
            P("ep", None, "tp"),
            P("ep", None, "tp"),
            P("ep", "tp", None),
            P("tp"),
        ),
        out_specs=P("ep", "tp"),
        check_vma=False,
    )
```

profile of v0, /device:TPU:0, one launch (start us, length us, event | category | flops | bytes accessed | tf_op | source)
XLA Modules:
  0.0 91.5 jit_solution(16629815895781907717)
XLA Ops:
  6.5 0.0 copy-start
  6.5 0.0 copy-start.3
  6.5 0.0 copy-start.12
  6.5 0.0 copy-start.13
  6.5 0.0 copy-start.11
  6.5 0.0 copy-start.8
  6.6 0.0 copy-start.2
  6.6 0.0 reduce-scatter.2.cloned.1.call-start
  6.6 0.0 copy-start.10
  6.6 1.0 %fusion.22 = f32[16]{0:T(128)S(1)} fusion(bf16[16,1024]{1,0:T(8,128)(2,1)} %param.21), kind=kLoop, calls=%fused_computation.38 | loop fusion | flops 49136 | bytes 32832 | tf_op jit(solution)/shard_map/reduce_sum | solution.py:10
  9.0 0.0 copy-start.4
  9.0 1.2 %convolution_multiply_fusion.2 = f32[16,128]{1,0:T(8,128)S(1)} fusion(bf16[1024,128]{1,0:T(8,128)(2,1)} %param.25, bf16[16,1024]{1,0:T(8,128)(2,1)} %param.21, f32[1024]{0:T(1024)} %param.24, f32[16]{0:T(128)S(1)} %add_rsqrt_fusion.4), kind=kOutput, calls=%fused_computation.14 | convolution fusion | flops 4261888 | bytes 307264 | tf_op jit(solution)/shard_map/dot_general | solution.py:44
  10.2 0.0 copy-start.5
  10.2 1.3 %fusion.6 = f32[16]{0:T(128)S(1)} fusion(f32[16,128]{1,0:T(8,128)S(1)} %convolution_multiply_fusion.2, bf16[1024,128]{1,0:T(8,128)(2,1)} %param.26, bf16[16,1024]{1,0:T(8,128)(2,1)} %param.21, f32[1024]{0:T(1024)} %param.24, f32[16]{0:T(128)S(1)} %add_rsqrt_fusion.4), kind=kOutput, calls=%fused_computation.15 | convolution fusion | flops 4263920 | bytes 307328 | tf_op jit(solution)/shard_map/dot_general | solution.py:47
  11.5 0.0 copy-start.7
  11.5 1.0 %fusion.8 = f32[16,1]{0,1:T(1,128)S(1)} fusion(bf16[1024,1]{0,1:T(2,128)(2,1)} %param.28, f32[]{:T(128)} %bitcast.97, bf16[16,1024]{1,0:T(8,128)(2,1)} %param.21, f32[1024]{0:T(1024)} %param.24, f32[16]{0:T(128)S(1)} %add_rsqrt_fusion.4), kind=kOutput, calls=%fused_computation.18 | convolution fusion | flops 98320 | bytes 39044 | tf_op jit(solution)/shard_map/dot_general | solution.py:49
  12.5 0.0 copy-done
  12.5 0.0 copy-start.1
  12.5 1.1 %fusion = f32[16,1,256]{2,1,0:T(1,128)S(1)} fusion(f32[16,128,1]{1,2,0:T(1,128)S(1)} %bitcast.101, f32[16,1,128,256]{3,2,1,0:T(8,128)S(1)} %copy-done), kind=kOutput, calls=%fused_computation.1 | convolution fusion | flops 6291456 | bytes 2121728 | tf_op jit(solution)/shard_map/shk,shkv->shv/dot_general | solution.py:57
  13.6 0.0 copy-done.3
  13.6 0.0 copy-done.12
  13.6 0.0 copy-done.13
  13.6 0.0 copy-done.11
  13.6 0.2 fusion.39
  13.9 0.0 copy-done.10
  13.9 0.3 multiply_reduce_fusion.3
  14.2 0.0 copy-done.8
  14.2 0.0 copy-done.2
  14.2 0.2 convolution_convert_fusion.2
  14.5 12.9 %psum.14 = bf16[16,1024]{1,0:T(8,128)(2,1)S(1)} all-reduce(bf16[16,1024]{1,0:T(8,128)(2,1)S(1)} %convolution_convert_fusion.2), channel_id=1, replica_groups=mesh['ep'=8,'tp'=4] {'tp'}, use_global_device_ids=true, to_apply=%region_3.4 | all-reduce | flops 16384 | bytes 65536 | tf_op jit(solution)/shard_map/psum | solution.py:66
  27.4 0.1 fusion.20
  27.5 0.0 copy-done.4
  27.5 0.2 multiply_reduce_fusion.1
  27.7 0.0 copy-start.6
  27.8 0.0 copy-done.5
  27.8 0.1 copy.29
  27.8 0.1 reshape.181
  27.9 0.1 fusion.27
  28.0 0.1 reduce_window_sum.11
  28.2 0.2 select_reduce_fusion
  28.3 0.1 reduce_sum.84
  28.5 0.1 copy.31
  28.5 0.1 fusion.28
  28.6 0.0 copy-done.7
  28.6 0.3 convolution_convert_fusion.1
  28.9 0.0 copy-start.9
  28.9 13.8 %all_to_all.10 = bf16[8,16,1024]{2,1,0:T(8,128)(2,1)S(1)} all-to-all(bf16[8,16,1024]{2,1,0:T(8,128)(2,1)S(1)} %bitcast.100), channel_id=1, replica_groups=mesh['ep'=8,'tp'=4] {'ep'}, dimensions={0} | all-to-all | bytes 524288 | tf_op jit(solution)/shard_map/all_to_all | solution.py:90
  42.8 0.0 copy-done.1
  42.8 0.2 convolution_bitcast_fusion.1
  43.0 2.4 %convolution_convert_fusion = bf16[8,16,1024]{2,1,0:T(8,128)(2,1)} fusion(bf16[8,16,1024]{2,1,0:T(8,128)(2,1)S(1)} %all_to_all.10, bf16[1,256,1024]{2,1,0:T(8,128)(2,1)} %param.40, bf16[1,1024,256]{2,1,0:T(8,128)(2,1)} %param.39, f32[8,1,16,256]{3,2,0,1:T(8,128)S(1)} %convolution_bitcast_fusion.1), kind=kOutput, calls=%fused_computation.3 | convolution fusion | flops 134545408 | bytes 1703936 | tf_op jit(solution)/shard_map/secf,efd->secd/dot_general | solution.py:96
  45.4 0.0 reduce-scatter.2.cloned.1.call-update
  45.4 0.1 mul.213
  45.5 19.0 %reduce-scatter.2.cloned.1.call-done = bf16[8,16,256]{2,1,0:T(8,128)(2,1)} async-done(((bf16[8,16,1024]{2,1,0:T(8,128)(2,1)}), bf16[8,16,256]{2,1,0:T(8,128)(2,1)}) %reduce-scatter.2.cloned.1.call-update) | async-done | bytes 65552 | tf_op jit(solution)/shard_map/reduce_scatter | solution.py:99
  64.5 5.5 %all-to-all-start.1 = ((bf16[8,16,256]{2,1,0:T(8,128)(2,1)}), bf16[8,16,256]{2,1,0:T(8,128)(2,1)S(1)}, u32[]{:S(2)}, u32[]{:S(2)}) async-start(bf16[8,16,256]{2,1,0:T(8,128)(2,1)} %reduce-scatter.2.cloned.1.call-done), calls=%async_computation.2 | async-start | bytes 131072 | tf_op jit(solution)/shard_map/all_to_all | solution.py:103
  70.1 0.0 copy-done.6
  70.1 0.1 copy.28
  70.2 6.8 %all-to-all-done.1 = bf16[8,16,256]{2,1,0:T(8,128)(2,1)S(1)} async-done(((bf16[8,16,256]{2,1,0:T(8,128)(2,1)}), bf16[8,16,256]{2,1,0:T(8,128)(2,1)S(1)}, u32[]{:S(2)}, u32[]{:S(2)}) %all-to-all-start.1) | async-done | bytes 65568 | tf_op jit(solution)/shard_map/all_to_all | solution.py:103
  77.0 0.8 gather_fusion
  77.8 0.1 multiply_reduce_fusion
  77.9 0.1 multiply_reduce_fusion.2
  78.0 5.9 %psum.15 = f32[16]{0:T(128)S(1)} all-reduce(f32[16]{0:T(128)S(1)} %multiply_reduce_fusion.2), channel_id=1, replica_groups=mesh['ep'=8,'tp'=4] {'tp'}, use_global_device_ids=true, to_apply=%region_12.13 | all-reduce | flops 16 | bytes 128 | tf_op jit(solution)/shard_map/psum | solution.py:110
  84.0 0.0 copy-done.9
  84.0 0.7 add_convert_fusion
  (10 shorter events, 0.1 us)
Async XLA Ops:
  6.5 6.0 %copy-start = (f32[16,1,128,256]{3,2,1,0:T(8,128)S(1)}, f32[16,1,128,256]{3,2,1,0:T(8,128)}, u32[]{:S(2)}) copy-start(f32[16,1,128,256]{3,2,1,0:T(8,128)} %param.22) | copy-start | bytes 6291460
  6.5 7.1 %copy-start.3 = (bf16[16,1024]{1,0:T(8,128)(2,1)S(1)}, bf16[16,1024]{1,0:T(8,128)(2,1)}, u32[]{:S(2)}) copy-start(bf16[16,1024]{1,0:T(8,128)(2,1)} %param.21) | copy-start | bytes 98308
  6.5 7.1 %copy-start.12 = (f32[1024]{0:T(1024)S(1)}, f32[1024]{0:T(1024)}, u32[]{:S(2)}) copy-start(f32[1024]{0:T(1024)} %param.24) | copy-start | bytes 12292
  6.5 7.1 %copy-start.13 = (f32[16,1]{0,1:T(1,128)S(1)}, f32[16,1]{0,1:T(1,128)}, u32[]{:S(2)}) copy-start(f32[16,1]{0,1:T(1,128)} %param.23) | copy-start | bytes 196
  6.5 7.1 %copy-start.11 = (bf16[1024,1]{0,1:T(2,128)(2,1)S(1)}, bf16[1024,1]{0,1:T(2,128)(2,1)}, u32[]{:S(2)}) copy-start(bf16[1024,1]{0,1:T(2,128)(2,1)} %param.29) | copy-start | bytes 6148
  6.5 7.7 %copy-start.8 = (f32[256]{0:T(256)S(1)}, f32[256]{0:T(256)}, u32[]{:S(2)}) copy-start(f32[256]{0:T(256)} %param.32) | copy-start | bytes 3076
  6.6 7.7 %copy-start.2 = (bf16[256,1024]{1,0:T(8,128)(2,1)S(1)}, bf16[256,1024]{1,0:T(8,128)(2,1)}, u32[]{:S(2)}) copy-start(bf16[256,1024]{1,0:T(8,128)(2,1)} %param.33) | copy-start | bytes 1572868
  6.6 58.0 %reduce-scatter.2.cloned.1.call-start = ((), (), s32[]{:S(2)}) async-start(), calls=%async_computation.3 | async-start | bytes 327680 | tf_op jit(solution)/shard_map/reduce_scatter | solution.py:99
  6.6 7.3 %copy-start.10 = (bf16[1024,256]{1,0:T(8,128)(2,1)S(1)}, bf16[1024,256]{1,0:T(8,128)(2,1)}, u32[]{:S(2)}) copy-start(bf16[1024,256]{1,0:T(8,128)(2,1)} %param.27) | copy-start | bytes 1572868
  9.0 18.5 %copy-start.4 = (f32[1024]{0:T(1024)S(1)}, f32[1024]{0:T(1024)}, u32[]{:S(2)}) copy-start(f32[1024]{0:T(1024)} %param.34) | copy-start | bytes 12292
  10.2 17.6 %copy-start.5 = (s32[16,6]{0,1:T(8,128)S(1)}, s32[16,6]{0,1:T(8,128)}, u32[]{:S(2)}) copy-start(s32[16,6]{0,1:T(8,128)} %param.36) | copy-start | bytes 1156
  11.5 17.1 %copy-start.7 = (f32[1024]{0:T(1024)S(1)}, f32[1024]{0:T(1024)}, u32[]{:S(2)}) copy-start(f32[1024]{0:T(1024)} %param.35) | copy-start | bytes 12292
  12.5 30.2 %copy-start.1 = (bf16[1,1024,256]{2,1,0:T(8,128)(2,1)S(1)}, bf16[1,1024,256]{2,1,0:T(8,128)(2,1)}, u32[]{:S(2)}) copy-start(bf16[1,1024,256]{2,1,0:T(8,128)(2,1)} %param.38) | copy-start | bytes 1572868
  27.7 42.3 %copy-start.6 = (f32[16,6]{0,1:T(8,128)S(1)}, f32[16,6]{0,1:T(8,128)}, u32[]{:S(2)}) copy-start(f32[16,6]{0,1:T(8,128)} %param.37) | copy-start | bytes 1156
  28.9 55.0 %copy-start.9 = (f32[256]{0:T(256)S(1)}, f32[256]{0:T(256)}, u32[]{:S(2)}) copy-start(f32[256]{0:T(256)} %param.41) | copy-start | bytes 3076
  64.5 12.4 %all-to-all-start.1 = ((bf16[8,16,256]{2,1,0:T(8,128)(2,1)}), bf16[8,16,256]{2,1,0:T(8,128)(2,1)S(1)}, u32[]{:S(2)}, u32[]{:S(2)}) async-start(bf16[8,16,256]{2,1,0:T(8,128)(2,1)} %reduce-scatter.2.cloned.1.call-done), calls=%async_computation.2 | async-start | bytes 131072 | tf_op jit(solution)/shard_map/all_to_all | solution.py:103
Sparse Core Ops, SparseCore 0:
  45.5 18.9 reduce-scatter.1
where the time goes:
time: 91.9 us; the launch traced here: 91.5 us
  blocking collectives  32.7 us (36%)
  waiting for transfers between devices  25.8 us (28%)
  between operations  15 us (16%)
  matrix products  8.26 us (9%)
  starting transfers between devices  5.57 us (6%)
  other arithmetic  2.83 us (3%)
  local copies, waits for them, and re-layouts  1.35 us (1%)
    reduce_scatter x1, waiting for transfers between devices, per_device(): lax.psum_scatter(part.astype(jnp.bfloat16), 'tp', scatter_dimension=2, ti...  19 us
    all_to_all x1, blocking collectives, per_device(): lax.all_to_all(outbound, 'ep', split_axis=0, concat_axis=0, tiled=True)  13.8 us
    psum x1, blocking collectives, per_device(): lax.psum(partial_value.astype(jnp.bfloat16), 'tp').astype(jnp.float32)  12.9 us
    all_to_all x1, waiting for transfers between devices, per_device(): lax.all_to_all(done, 'ep', split_axis=0, concat_axis=0, tiled=True)  6.79 us
    psum x1, blocking collectives, per_device(): total = lax.psum(jnp.sum(routed * routed, axis=1), 'tp')  5.95 us
    all_to_all x1, starting transfers between devices, per_device(): lax.all_to_all(done, 'ep', split_axis=0, concat_axis=0, tiled=True)  5.53 us
    dot_general x1, matrix products, per_device(): jnp.einsum('secf,efd->secd', act, expert_down, preferred_element_type=f32)  2.4 us
  transfers between devices with their start and end apart: 2, of which 2 were waited for; matrix products, arithmetic and copies ran while one was open for 0% of the time, Pallas kernels for 0%

commit v1 on v0

--- a/solution.py
+++ b/solution.py
@@ -1,6 +1,10 @@
+import functools
+
 import jax
 import jax.numpy as jnp
 from jax import lax
+from jax.experimental import pallas as pl
+from jax.experimental.pallas import tpu as pltpu
 from jax.sharding import PartitionSpec as P
 
 EPS = 1e-06
@@ -10,7 +14,7 @@
     return lax.rsqrt(jnp.mean(values * values, axis=-1, keepdims=True) + EPS)
 
 
-def per_device(
+def routed_device(
     tokens,
     memory,
     log_scale,
@@ -112,6 +116,372 @@
     return (resid_part + scaled * ffn_gain_out).astype(bf16)
 
 
+F32 = jnp.float32
+BF16 = jnp.bfloat16
+MESH = pl.DeviceIdType.MESH
+
+
+def column_of(row):
+    n = row.shape[1]
+    eye = lax.broadcasted_iota(jnp.int32, (n, n), 0) == lax.broadcasted_iota(jnp.int32, (n, n), 1)
+    return jnp.sum(jnp.where(eye, jnp.broadcast_to(row, (n, n)), 0.0), axis=1, keepdims=True)
+
+
+def layer_kernel(
+    groups,
+    lanes,
+    tokens_hbm,
+    memory_hbm,
+    log_scale_ref,
+    gain_in_ref,
+    w_query_hbm,
+    w_key_hbm,
+    w_value_hbm,
+    w_igate_ref,
+    w_fgate_ref,
+    igate_bias_ref,
+    fgate_bias_ref,
+    head_gain_ref,
+    w_output_hbm,
+    gain_out_ref,
+    ffn_gain_ref,
+    routes_ref,
+    route_weights_ref,
+    gate_hbm,
+    up_hbm,
+    down_hbm,
+    ffn_gain_out_ref,
+    out_ref,
+    tokens_v,
+    memory_v,
+    w_query_v,
+    w_key_v,
+    w_value_v,
+    w_output_v,
+    gate_v,
+    up_v,
+    down_v,
+    recall_v,
+    shares,
+    rows,
+    resid_v,
+    parts,
+    results,
+    squares,
+    load_sem,
+    memory_sem,
+    share_send,
+    share_recv,
+    rows_send,
+    rows_recv,
+    parts_send,
+    parts_recv,
+    squares_send,
+    squares_recv,
+):
+    ep = lax.axis_index("ep")
+    tp = lax.axis_index("tp")
+    seqs, width = tokens_v.shape
+    key_dim = memory_v.shape[1]
+    value_dim = memory_v.shape[2]
+    quarter = width // lanes
+
+    def device(off, toff):
+        return (lax.rem(ep + (off % groups), groups), lax.rem(tp + (toff % lanes), lanes))
+
+    pieces = memory_sem.shape[0]
+    piece = seqs // pieces
+    loads = {}
+    for i, (name, src, dst) in enumerate(
+        (
+            ("tokens", tokens_hbm, tokens_v),
+            ("query", w_query_hbm, w_query_v),
+            ("key", w_key_hbm, w_key_v),
+            ("value", w_value_hbm, w_value_v),
+            ("output", w_output_hbm, w_output_v),
+            ("gate", gate_hbm.at[0], gate_v),
+            ("up", up_hbm.at[0], up_v),
+            ("down", down_hbm.at[0], down_v),
+        )
+    ):
+        loads[name] = pltpu.make_async_copy(src, dst, load_sem.at[i])
+    memory_loads = [
+        pltpu.make_async_copy(
+            memory_hbm.at[pl.ds(i * piece, piece), 0],
+            memory_v.at[pl.ds(i * piece, piece)],
+            memory_sem.at[i],
+        )
+        for i in range(pieces)
+    ]
+    for name in ("tokens", "query", "key", "value"):
+        loads[name].start()
+    for load in memory_loads:
+        load.start()
+    for name in ("output", "gate", "up", "down"):
+        loads[name].start()
+
+    barrier = pltpu.get_barrier_semaphore()
+    for off in range(groups):
+        for toff in range(lanes):
+            if off or toff:
+                pl.semaphore_signal(
+                    barrier, inc=1, device_id=device(off, toff), device_id_type=MESH
+                )
+
+    loads["tokens"].wait()
+    xf = tokens_v[...].astype(F32)
+    normed = (xf * rms_scale(xf) * gain_in_ref[...]).astype(BF16)
+    nf = normed.astype(F32)
+    in_pre = (
+        jnp.sum(nf * w_igate_ref[...].astype(F32), axis=1, keepdims=True) + igate_bias_ref[...]
+    )
+    fpre = jnp.sum(nf * w_fgate_ref[...].astype(F32), axis=1, keepdims=True) + fgate_bias_ref[...]
+    forget_log = jnp.minimum(fpre, 0.0) - jnp.log1p(jnp.exp(-jnp.abs(fpre)))
+    carried = forget_log + column_of(log_scale_ref[...])
+    new_max = jnp.maximum(carried, in_pre)
+    carry_weight = jnp.exp(carried - new_max)
+    fresh_weight = jnp.exp(in_pre - new_max)
+    loads["query"].wait()
+    query = jnp.dot(normed, w_query_v[...], preferred_element_type=F32) * key_dim ** (-0.5)
+    loads["key"].wait()
+    keys = jnp.dot(normed, w_key_v[...], preferred_element_type=F32)
+    loads["value"].wait()
+    values = jnp.dot(normed, w_value_v[...], preferred_element_type=F32)
+    match = jnp.sum(query * keys, axis=1, keepdims=True)
+    turned = query.T
+    for i in range(pieces):
+        memory_loads[i].wait()
+        for s in range(i * piece, (i + 1) * piece):
+            recall_v[s : s + 1, :] = jnp.sum(
+                turned[:, s : s + 1] * memory_v[s], axis=0, keepdims=True
+            )
+    read = carry_weight * recall_v[...] + (fresh_weight * match) * values
+    headout = (read * rms_scale(read) * head_gain_ref[...]).astype(BF16)
+    loads["output"].wait()
+    shares[0] = jnp.dot(headout, w_output_v[...], preferred_element_type=F32).astype(BF16)
+
+    pl.semaphore_wait(barrier, groups * lanes - 1)
+    copies = []
+    for toff in range(1, lanes):
+        copy = pltpu.make_async_remote_copy(
+            src_ref=shares.at[0],
+            dst_ref=shares.at[toff],
+            send_sem=share_send.at[toff],
+            recv_sem=share_recv.at[toff],
+            device_id=device(0, toff),
+            device_id_type=MESH,
+        )
+        copy.start()
+        copies.append(copy)
+    mine = [
+        column_of(
+            jnp.sum(
+                jnp.where(
+                    routes_ref[...] == lax.rem(ep + off, groups), route_weights_ref[...], 0.0
+                ),
+                axis=0,
+                keepdims=True,
+            )
+        )
+        for off in range(groups)
+    ]
+    mixed = shares[0].astype(F32)
+    for toff in range(1, lanes):
+        copies[toff - 1].wait_recv()
+        mixed = mixed + shares[toff].astype(F32)
+    resid = (xf + mixed * rms_scale(mixed) * gain_out_ref[...]).astype(BF16)
+    rf = resid.astype(F32)
+    rows[0] = (rf * rms_scale(rf) * ffn_gain_ref[...]).astype(BF16)
+    for off in range(1, groups):
+        copy = pltpu.make_async_remote_copy(
+            src_ref=rows.at[0],
+            dst_ref=rows.at[off],
+            send_sem=rows_send.at[off],
+            recv_sem=rows_recv.at[off],
+            device_id=device(off, 0),
+            device_id_type=MESH,
+        )
+        copy.start()
+        copies.append(copy)
+    for q in range(lanes):
+        resid_v[q] = rf[:, q * quarter : (q + 1) * quarter]
+
+    loads["gate"].wait()
+    loads["up"].wait()
+    loads["down"].wait()
+    for copy in copies[lanes - 1 :]:
+        copy.wait_recv()
+    x = rows[...].reshape(groups * seqs, width)
+    gate = jnp.dot(x, gate_v[...], preferred_element_type=F32)
+    up = jnp.dot(x, up_v[...], preferred_element_type=F32)
+    act = (jax.nn.silu(gate) * up).astype(BF16)
+    for q in range(lanes):
+        parts[q] = (
+            jnp.dot(
+                act, down_v[:, q * quarter : (q + 1) * quarter], preferred_element_type=F32
+            )
+            .astype(BF16)
+            .reshape(groups, seqs, quarter)
+        )
+    back = {}
+    for off in range(groups):
+        for toff in range(lanes):
+            src = parts.at[lax.rem(tp + toff, lanes), off]
+            if off or toff:
+                back[off, toff] = pltpu.make_async_remote_copy(
+                    src_ref=src,
+                    dst_ref=results.at[off, toff],
+                    send_sem=parts_send.at[off, toff],
+                    recv_sem=parts_recv.at[off, toff],
+                    device_id=device(-off, toff),
+                    device_id_type=MESH,
+                )
+                back[off, toff].start()
+
+    routed = None
+    for off in range(groups):
+        total = None
+        for toff in range(lanes):
+            if off or toff:
+                back[off, toff].wait_recv()
+                part = results[off, toff]
+            else:
+                part = parts[tp, 0]
+            part = part.astype(F32)
+            total = part if total is None else total + part
+        term = mine[off] * total.astype(BF16).astype(F32)
+        routed = term if routed is None else routed + term
+    squares[0] = jnp.broadcast_to(
+        jnp.sum(routed * routed, axis=1, keepdims=True), squares.shape[1:]
+    )
+    last = []
+    for toff in range(1, lanes):
+        copy = pltpu.make_async_remote_copy(
+            src_ref=squares.at[0],
+            dst_ref=squares.at[toff],
+            send_sem=squares_send.at[toff],
+            recv_sem=squares_recv.at[toff],
+            device_id=device(0, toff),
+            device_id_type=MESH,
+        )
+        copy.start()
+        last.append(copy)
+    for copy in copies:
+        copy.wait_send()
+    for copy in back.values():
+        copy.wait_send()
+    total = squares[0]
+    for toff in range(1, lanes):
+        last[toff - 1].wait_recv()
+        total = total + squares[toff]
+    scaled = routed * lax.rsqrt(total[:, :1] / width + EPS)
+    out_ref[...] = (resid_v[tp] + scaled * ffn_gain_out_ref[...]).astype(BF16)
+    for copy in last:
+        copy.wait_send()
+
+
+def per_device(*args):
+    (
+        tokens,
+        memory,
+        log_scale,
+        mix_gain_in,
+        w_query,
+        w_key,
+        w_value,
+        w_igate,
+        w_fgate,
+        igate_bias,
+        fgate_bias,
+        head_gain,
+        w_output,
+        mix_gain_out,
+        ffn_gain_in,
+        routes,
+        route_weights,
+        expert_gate,
+        expert_up,
+        expert_down,
+        ffn_gain_out,
+    ) = args
+    groups = lax.axis_size("ep")
+    lanes = lax.axis_size("tp")
+    seqs, width = tokens.shape
+    local_experts, _, hidden = expert_gate.shape
+    top = routes.shape[1]
+    if local_experts != 1 or log_scale.shape[1] != 1 or 2 * top < groups:
+        return routed_device(*args)
+    quarter = width // lanes
+    key_dim, value_dim = memory.shape[2:]
+    vmem = pl.BlockSpec(memory_space=pltpu.VMEM)
+    hbm = pl.BlockSpec(memory_space=pl.ANY)
+    dma = pltpu.SemaphoreType.DMA
+    pieces = 4 if seqs % 4 == 0 else 1
+    operands = (
+        (tokens, hbm),
+        (memory, hbm),
+        (log_scale.T, vmem),
+        (mix_gain_in.reshape(1, -1), vmem),
+        (w_query, hbm),
+        (w_key, hbm),
+        (w_value, hbm),
+        (w_igate.T, vmem),
+        (w_fgate.T, vmem),
+        (igate_bias.reshape(1, 1), vmem),
+        (fgate_bias.reshape(1, 1), vmem),
+        (head_gain.reshape(1, -1), vmem),
+        (w_output, hbm),
+        (mix_gain_out.reshape(1, -1), vmem),
+        (ffn_gain_in.reshape(1, -1), vmem),
+        (routes.T, vmem),
+        (route_weights.T, vmem),
+        (expert_gate, hbm),
+        (expert_up, hbm),
+        (expert_down, hbm),
+        (ffn_gain_out.reshape(1, -1), vmem),
+    )
+    return pl.pallas_call(
+        functools.partial(layer_kernel, groups, lanes),
+        out_shape=jax.ShapeDtypeStruct((seqs, quarter), BF16),
+        in_specs=[spec for _, spec in operands],
+        out_specs=vmem,
+        scratch_shapes=[
+            pltpu.VMEM((seqs, width), BF16),
+            pltpu.VMEM((seqs, key_dim, value_dim), F32),
+            pltpu.VMEM(w_query.shape, BF16),
+            pltpu.VMEM(w_key.shape, BF16),
+            pltpu.VMEM(w_value.shape, BF16),
+            pltpu.VMEM(w_output.shape, BF16),
+            pltpu.VMEM((width, hidden), BF16),
+            pltpu.VMEM((width, hidden), BF16),
+            pltpu.VMEM((hidden, width), BF16),
+            pltpu.VMEM((seqs, value_dim), F32),
+            pltpu.VMEM((lanes, seqs, width), BF16),
+            pltpu.VMEM((groups, seqs, width), BF16),
+            pltpu.VMEM((lanes, seqs, quarter), F32),
+            pltpu.VMEM((lanes, groups, seqs, quarter), BF16),
+            pltpu.VMEM((groups, lanes, seqs, quarter), BF16),
+            pltpu.VMEM((lanes, seqs, 128), F32),
+            dma((8,)),
+            dma((pieces,)),
+            dma((lanes,)),
+            dma((lanes,)),
+            dma((groups,)),
+            dma((groups,)),
+            dma((groups, lanes)),
+            dma((groups, lanes)),
+            dma((lanes,)),
+            dma((lanes,)),
+        ],
+        compiler_params=pltpu.CompilerParams(
+            collective_id=0,
+            has_side_effects=True,
+            vmem_limit_bytes=60 * 1024 * 1024,
+        ),
+        name="layer",
+    )(*[array for array, _ in operands])
+
+
 def solution(mesh):
     return jax.shard_map(
         per_device,

time: 91.9 us -> 34.3 us (0.37)
  blocking collectives: 32.7 us -> 0 us
  Pallas kernels: 0 us -> 31.5 us
  waiting for transfers between devices: 25.8 us -> 0 us
  between operations: 15 us -> 1.3 us
  matrix products: 8.26 us -> 0 us
  starting transfers between devices: 5.57 us -> 0 us
  other arithmetic: 2.83 us -> 0 us
    pallas_call x0 -> x1, Pallas kernels: none -> 31.5 us  [per_device(): pl.pallas_call(functools.partial(layer_kernel, groups, lanes), out_shape=...]
    reduce_scatter x1 -> x0, waiting for transfers between devices: 19 us -> none  [per_device(): lax.psum_scatter(part.astype(jnp.bfloat16), 'tp', scatter_dimension=2, ti...]
    psum x2 -> x0, blocking collectives: 18.9 us -> none  [the longest x1 12.9 us: per_device(): lax.psum(partial_value.astype(jnp.bfloat16), 'tp').astype(jnp.float32)]
    all_to_all x1 -> x0, blocking collectives: 13.8 us -> none  [per_device(): lax.all_to_all(outbound, 'ep', split_axis=0, concat_axis=0, tiled=True)]
    dot_general x10 -> x0, matrix products: 8.26 us -> none  [the longest x1 2.4 us: per_device(): jnp.einsum('secf,efd->secd', act, expert_down, preferred_element_type=f32)]
    all_to_all x1 -> x0, waiting for transfers between devices: 6.79 us -> none  [per_device(): lax.all_to_all(done, 'ep', split_axis=0, concat_axis=0, tiled=True)]
    all_to_all x1 -> x0, starting transfers between devices: 5.53 us -> none  [per_device(): lax.all_to_all(done, 'ep', split_axis=0, concat_axis=0, tiled=True)]
    reduce_sum x6 -> x0, other arithmetic: 1.77 us -> none  [the longest x3 1.36 us: rms_scale(): return lax.rsqrt(jnp.mean(values * values, axis=-1, keepdims=True) + EPS)]
  transfers between devices with their start and end apart: 2 -> 0, of which waited for: 2 -> 0; matrix products, arithmetic and copies ran while one was open for 0% -> 0% of each run, Pallas kernels for 0% -> 0%
where the time goes in v1:
time: 34.3 us; the launch traced here: 34.1 us
  Pallas kernels  31.5 us (92%)
  local copies, waits for them, and re-layouts  1.3 us (4%)
  between operations  1.3 us (4%)
    pallas_call x1, Pallas kernels, per_device(): pl.pallas_call(functools.partial(layer_kernel, groups, lanes), out_shape=...  31.5 us
    unnamed x1, local copies, waits for them, and re-layouts  1.3 us

profile of v1, /device:TPU:0, one launch (start us, length us, event | category | flops | bytes accessed | tf_op | source)
XLA Modules:
  0.0 34.1 jit_solution(2328637306942665972)
XLA Ops:
  1.3 31.5 %layer.1 = bf16[16,256]{1,0:T(8,128)(2,1)} custom-call(bf16[16,1024]{1,0:T(8,128)(2,1)} %tokens_hbm.1, f32[16,1,128,256]{3,2,1,0:T(8,128)} %memory_hbm.1, f32[1,16]{1,0:T(1,128)} %bitcast.23, f32[1,1024]{1,0:T(1,128)} %bitcast.14, bf16[1024,128]{1,0:T(8,128)(2,1)} %w_query_hbm.1, bf16[1024,128]{1,0:T(8,128)(2,1)} %w_key_hbm.1, ...), custom_call_target="tpu_custom_call" | custom-call | tf_op jit(solution)/shard_map/layer/pallas_call | solution.py:443
  32.8 1.3 %copy.25 = bf16[16,256]{1,0:T(8,128)(2,1)} copy(bf16[16,256]{1,0:T(8,128)(2,1)} %layer.1) | data formatting | bytes 16384

commit v2 on v1

--- a/solution.py
+++ b/solution.py
@@ -164,12 +164,15 @@
     recall_v,
     shares,
     rows,
+    inbox,
     resid_v,
     parts,
     results,
     squares,
     load_sem,
     memory_sem,
+    pair_send,
+    pair_recv,
     share_send,
     share_recv,
     rows_send,
@@ -185,6 +188,8 @@
     key_dim = memory_v.shape[1]
     value_dim = memory_v.shape[2]
     quarter = width // lanes
+    core, chip = lax.rem(tp, 2), tp // 2
+    slots, chips, half = groups // 2, lanes // 2, width // 2
 
     def device(off, toff):
         return (lax.rem(ep + (off % groups), groups), lax.rem(tp + (toff % lanes), lanes))
@@ -199,9 +204,9 @@
             ("key", w_key_hbm, w_key_v),
             ("value", w_value_hbm, w_value_v),
             ("output", w_output_hbm, w_output_v),
-            ("gate", gate_hbm.at[0], gate_v),
-            ("up", up_hbm.at[0], up_v),
-            ("down", down_hbm.at[0], down_v),
+            ("gate", gate_hbm.at[0], gate_v.at[0]),
+            ("up", up_hbm.at[0], up_v.at[0]),
+            ("down", down_hbm.at[0], down_v.at[0]),
         )
     ):
         loads[name] = pltpu.make_async_copy(src, dst, load_sem.at[i])
@@ -273,6 +278,19 @@
         )
         copy.start()
         copies.append(copy)
+    pairs = []
+    for i, (name, ref) in enumerate((("gate", gate_v), ("up", up_v), ("down", down_v))):
+        loads[name].wait()
+        copy = pltpu.make_async_remote_copy(
+            src_ref=ref.at[0],
+            dst_ref=ref.at[1],
+            send_sem=pair_send.at[i],
+            recv_sem=pair_recv.at[i],
+            device_id=(ep, tp + 1 - 2 * core),
+            device_id_type=MESH,
+        )
+        copy.start()
+        pairs.append(copy)
     mine = [
         column_of(
             jnp.sum(
@@ -291,14 +309,16 @@
         mixed = mixed + shares[toff].astype(F32)
     resid = (xf + mixed * rms_scale(mixed) * gain_out_ref[...]).astype(BF16)
     rf = resid.astype(F32)
-    rows[0] = (rf * rms_scale(rf) * ffn_gain_ref[...]).astype(BF16)
-    for off in range(1, groups):
+    ffn_in = (rf * rms_scale(rf) * ffn_gain_ref[...]).astype(BF16)
+    for h in range(2):
+        rows[h] = ffn_in[:, h * half : (h + 1) * half]
+    for off in range(groups - 1, 0, -1):
         copy = pltpu.make_async_remote_copy(
-            src_ref=rows.at[0],
-            dst_ref=rows.at[off],
+            src_ref=rows.at[core],
+            dst_ref=inbox.at[core, off // 2],
             send_sem=rows_send.at[off],
-            recv_sem=rows_recv.at[off],
-            device_id=device(off, 0),
+            recv_sem=rows_recv.at[core, off // 2],
+            device_id=(lax.rem(ep + off, groups), 2 * chip + off % 2),
             device_id_type=MESH,
         )
         copy.start()
@@ -306,53 +326,101 @@
     for q in range(lanes):
         resid_v[q] = rf[:, q * quarter : (q + 1) * quarter]
 
-    loads["gate"].wait()
-    loads["up"].wait()
-    loads["down"].wait()
-    for copy in copies[lanes - 1 :]:
+    def arrived(ref, sem):
+        pltpu.make_async_copy(ref, ref, sem).wait()
+
+    @pl.when(core == 0)
+    def _():
+        for h in range(2):
+            inbox[h, 0] = ffn_in[:, h * half : (h + 1) * half]
+
+    @pl.when(core == 1)
+    def _():
+        for h in range(2):
+            arrived(inbox.at[h, 0], rows_recv.at[h, 0])
+
+    for copy in pairs:
         copy.wait_recv()
-    x = rows[...].reshape(groups * seqs, width)
-    gate = jnp.dot(x, gate_v[...], preferred_element_type=F32)
-    up = jnp.dot(x, up_v[...], preferred_element_type=F32)
-    act = (jax.nn.silu(gate) * up).astype(BF16)
+    for slot in range(1, slots):
+        for h in range(2):
+            arrived(inbox.at[h, slot], rows_recv.at[h, slot])
+    x = [inbox[h].reshape(slots * seqs, half) for h in range(2)]
+
+    def into(weights, block):
+        return sum(
+            jnp.dot(
+                x[h], weights[block, h * half : (h + 1) * half, :], preferred_element_type=F32
+            )
+            for h in range(2)
+        )
+
+    act = [
+        (jax.nn.silu(into(gate_v, block)) * into(up_v, block)).astype(BF16) for block in range(2)
+    ]
     for q in range(lanes):
         parts[q] = (
-            jnp.dot(
-                act, down_v[:, q * quarter : (q + 1) * quarter], preferred_element_type=F32
+            sum(
+                jnp.dot(
+                    act[block],
+                    down_v[block, :, q * quarter : (q + 1) * quarter],
+                    preferred_element_type=F32,
+                )
+                for block in range(2)
             )
             .astype(BF16)
-            .reshape(groups, seqs, quarter)
-        )
-    back = {}
-    for off in range(groups):
-        for toff in range(lanes):
-            src = parts.at[lax.rem(tp + toff, lanes), off]
-            if off or toff:
-                back[off, toff] = pltpu.make_async_remote_copy(
-                    src_ref=src,
-                    dst_ref=results.at[off, toff],
-                    send_sem=parts_send.at[off, toff],
-                    recv_sem=parts_recv.at[off, toff],
-                    device_id=device(-off, toff),
-                    device_id_type=MESH,
-                )
-                back[off, toff].start()
+            .reshape(slots, seqs, quarter)
+        )
+
+    def result(slot, toff):
+        return pltpu.make_async_remote_copy(
+            src_ref=parts.at[lax.rem(tp + toff, lanes), slot],
+            dst_ref=results.at[2 * slot + core, chip],
+            send_sem=parts_send.at[slot, toff],
+            recv_sem=parts_recv.at[2 * slot + core, chip],
+            device_id=(
+                lax.rem(ep + groups - 2 * slot - core, groups),
+                lax.rem(tp + toff, lanes),
+            ),
+            device_id_type=MESH,
+        )
+
+    for slot in range(slots - 1, -1, -1):
+        for toff in range(lanes - 1, -1, -1):
+            if slot or toff:
+                result(slot, toff).start()
+
+    @pl.when(core == 1)
+    def _():
+        result(0, 0).start()
+
+    @pl.when(core == 0)
+    def _():
+        results[0, chip] = parts[tp, 0]
 
     routed = None
     for off in range(groups):
         total = None
-        for toff in range(lanes):
-            if off or toff:
-                back[off, toff].wait_recv()
-                part = results[off, toff]
+        for y in range(chips):
+            if off:
+                arrived(results.at[off, y], parts_recv.at[off, y])
             else:
-                part = parts[tp, 0]
-            part = part.astype(F32)
+
+                @pl.when((core == 1) | (chip != y))
+                def _():
+                    arrived(results.at[off, y], parts_recv.at[off, y])
+
+            part = results[off, y].astype(F32)
             total = part if total is None else total + part
         term = mine[off] * total.astype(BF16).astype(F32)
         routed = term if routed is None else routed + term
-    squares[0] = jnp.broadcast_to(
-        jnp.sum(routed * routed, axis=1, keepdims=True), squares.shape[1:]
+    wide = squares.shape[2]
+    eye = lax.broadcasted_iota(jnp.int32, (seqs, wide), 0) == lax.broadcasted_iota(
+        jnp.int32, (seqs, wide), 1
+    )
+    squares[0] = jnp.sum(
+        jnp.where(eye, jnp.sum(routed * routed, axis=1, keepdims=True), 0.0),
+        axis=0,
+        keepdims=True,
     )
     last = []
     for toff in range(1, lanes):
@@ -368,13 +436,25 @@
         last.append(copy)
     for copy in copies:
         copy.wait_send()
-    for copy in back.values():
+    for copy in pairs:
         copy.wait_send()
+    for slot in range(slots):
+        for toff in range(lanes):
+            if slot or toff:
+                result(slot, toff).wait_send()
+
+    @pl.when(core == 1)
+    def _():
+        result(0, 0).wait_send()
+
     total = squares[0]
     for toff in range(1, lanes):
         last[toff - 1].wait_recv()
         total = total + squares[toff]
-    scaled = routed * lax.rsqrt(total[:, :1] / width + EPS)
+    scale = jnp.sum(
+        jnp.where(eye, lax.rsqrt(total / width + EPS), 0.0), axis=1, keepdims=True
+    )
+    scaled = routed * scale
     out_ref[...] = (resid_v[tp] + scaled * ffn_gain_out_ref[...]).astype(BF16)
     for copy in last:
         copy.wait_send()
@@ -409,7 +489,7 @@
     seqs, width = tokens.shape
     local_experts, _, hidden = expert_gate.shape
     top = routes.shape[1]
-    if local_experts != 1 or log_scale.shape[1] != 1 or 2 * top < groups:
+    if local_experts != 1 or log_scale.shape[1] != 1 or 2 * top < groups or groups % 2 or lanes % 2:
         return routed_device(*args)
     quarter = width // lanes
     key_dim, value_dim = memory.shape[2:]
@@ -452,24 +532,27 @@
             pltpu.VMEM(w_key.shape, BF16),
             pltpu.VMEM(w_value.shape, BF16),
             pltpu.VMEM(w_output.shape, BF16),
-            pltpu.VMEM((width, hidden), BF16),
-            pltpu.VMEM((width, hidden), BF16),
-            pltpu.VMEM((hidden, width), BF16),
+            pltpu.VMEM((2, width, hidden), BF16),
+            pltpu.VMEM((2, width, hidden), BF16),
+            pltpu.VMEM((2, hidden, width), BF16),
             pltpu.VMEM((seqs, value_dim), F32),
             pltpu.VMEM((lanes, seqs, width), BF16),
-            pltpu.VMEM((groups, seqs, width), BF16),
+            pltpu.VMEM((2, seqs, width // 2), BF16),
+            pltpu.VMEM((2, groups // 2, seqs, width // 2), BF16),
             pltpu.VMEM((lanes, seqs, quarter), F32),
-            pltpu.VMEM((lanes, groups, seqs, quarter), BF16),
-            pltpu.VMEM((groups, lanes, seqs, quarter), BF16),
-            pltpu.VMEM((lanes, seqs, 128), F32),
+            pltpu.VMEM((lanes, groups // 2, seqs, quarter), BF16),
+            pltpu.VMEM((groups, lanes // 2, seqs, quarter), BF16),
+            pltpu.VMEM((lanes, 1, 128), F32),
             dma((8,)),
             dma((pieces,)),
+            dma((3,)),
+            dma((3,)),
             dma((lanes,)),
             dma((lanes,)),
             dma((groups,)),
-            dma((groups,)),
-            dma((groups, lanes)),
-            dma((groups, lanes)),
+            dma((2, groups // 2)),
+            dma((groups // 2, lanes)),
+            dma((groups, lanes // 2)),
             dma((lanes,)),
             dma((lanes,)),
         ],

time: 34.3 us -> 28 us (0.82)
  Pallas kernels: 31.5 us -> 25.1 us
    pallas_call x1, Pallas kernels: 31.5 us -> 25.1 us  [per_device(): pl.pallas_call(functools.partial(layer_kernel, groups, lanes), out_shape=...]
where the time goes in v2:
time: 28 us; the launch traced here: 27.7 us
  Pallas kernels  25.1 us (90%)
  local copies, waits for them, and re-layouts  1.3 us (5%)
  between operations  1.3 us (5%)
    pallas_call x1, Pallas kernels, per_device(): pl.pallas_call(functools.partial(layer_kernel, groups, lanes), out_shape=...  25.1 us
    unnamed x1, local copies, waits for them, and re-layouts  1.3 us

profile of v2, /device:TPU:0, one launch (start us, length us, event | category | flops | bytes accessed | tf_op | source)
XLA Modules:
  0.0 27.7 jit_solution(17614209547081327278)
XLA Ops:
  1.3 25.1 %layer.1 = bf16[16,256]{1,0:T(8,128)(2,1)} custom-call(bf16[16,1024]{1,0:T(8,128)(2,1)} %tokens_hbm.1, f32[16,1,128,256]{3,2,1,0:T(8,128)} %memory_hbm.1, f32[1,16]{1,0:T(1,128)} %bitcast.23, f32[1,1024]{1,0:T(1,128)} %bitcast.14, bf16[1024,128]{1,0:T(8,128)(2,1)} %w_query_hbm.1, bf16[1024,128]{1,0:T(8,128)(2,1)} %w_key_hbm.1, ...), custom_call_target="tpu_custom_call" | custom-call | tf_op jit(solution)/shard_map/layer/pallas_call | solution.py:523
  26.4 1.3 %copy.25 = bf16[16,256]{1,0:T(8,128)(2,1)} copy(bf16[16,256]{1,0:T(8,128)(2,1)} %layer.1) | data formatting | bytes 16384

commit v3 on v2

--- a/solution.py
+++ b/solution.py
@@ -132,26 +132,37 @@
     lanes,
     tokens_hbm,
     memory_hbm,
-    log_scale_ref,
-    gain_in_ref,
+    log_scale_hbm,
+    gain_in_hbm,
     w_query_hbm,
     w_key_hbm,
     w_value_hbm,
+    w_igate_hbm,
+    w_fgate_hbm,
+    igate_bias_ref,
+    fgate_bias_ref,
+    head_gain_hbm,
+    w_output_hbm,
+    gain_out_hbm,
+    ffn_gain_hbm,
+    routes_hbm,
+    route_weights_hbm,
+    gate_hbm,
+    up_hbm,
+    down_hbm,
+    ffn_gain_out_hbm,
+    out_ref,
+    log_scale_ref,
+    gain_in_ref,
     w_igate_ref,
     w_fgate_ref,
-    igate_bias_ref,
-    fgate_bias_ref,
     head_gain_ref,
-    w_output_hbm,
     gain_out_ref,
     ffn_gain_ref,
     routes_ref,
     route_weights_ref,
-    gate_hbm,
-    up_hbm,
-    down_hbm,
     ffn_gain_out_ref,
-    out_ref,
+    small_sem,
     tokens_v,
     memory_v,
     w_query_v,
@@ -194,6 +205,21 @@
     def device(off, toff):
         return (lax.rem(ep + (off % groups), groups), lax.rem(tp + (toff % lanes), lanes))
 
+    barrier = pltpu.get_barrier_semaphore()
+    for off in range(groups):
+        for toff in range(lanes):
+            if off or toff:
+                pl.semaphore_signal(
+                    barrier, inc=1, device_id=device(off, toff), device_id_type=MESH
+                )
+
+    def partner(off):
+        index, bit = 0, 1
+        while bit < groups:
+            index += bit * lax.rem(ep // bit + off // bit, 2)
+            bit *= 2
+        return index
+
     pieces = memory_sem.shape[0]
     piece = seqs // pieces
     loads = {}
@@ -218,29 +244,43 @@
         )
         for i in range(pieces)
     ]
-    for name in ("tokens", "query", "key", "value"):
+    small = [
+        pltpu.make_async_copy(src, dst, small_sem.at[i])
+        for i, (src, dst) in enumerate(
+            (
+                (log_scale_hbm, log_scale_ref),
+                (gain_in_hbm, gain_in_ref),
+                (w_igate_hbm, w_igate_ref),
+                (w_fgate_hbm, w_fgate_ref),
+                (head_gain_hbm, head_gain_ref),
+                (gain_out_hbm, gain_out_ref),
+                (ffn_gain_hbm, ffn_gain_ref),
+                (routes_hbm, routes_ref),
+                (route_weights_hbm, route_weights_ref),
+                (ffn_gain_out_hbm, ffn_gain_out_ref),
+            )
+        )
+    ]
+    loads["tokens"].start()
+    for load in small:
+        load.start()
+    for name in ("query", "key", "value"):
         loads[name].start()
     for load in memory_loads:
         load.start()
     for name in ("output", "gate", "up", "down"):
         loads[name].start()
 
-    barrier = pltpu.get_barrier_semaphore()
-    for off in range(groups):
-        for toff in range(lanes):
-            if off or toff:
-                pl.semaphore_signal(
-                    barrier, inc=1, device_id=device(off, toff), device_id_type=MESH
-                )
-
     loads["tokens"].wait()
+    for load in small:
+        load.wait()
     xf = tokens_v[...].astype(F32)
     normed = (xf * rms_scale(xf) * gain_in_ref[...]).astype(BF16)
     nf = normed.astype(F32)
     in_pre = (
-        jnp.sum(nf * w_igate_ref[...].astype(F32), axis=1, keepdims=True) + igate_bias_ref[...]
-    )
-    fpre = jnp.sum(nf * w_fgate_ref[...].astype(F32), axis=1, keepdims=True) + fgate_bias_ref[...]
+        jnp.sum(nf * w_igate_ref[...].astype(F32), axis=1, keepdims=True) + igate_bias_ref[0]
+    )
+    fpre = jnp.sum(nf * w_fgate_ref[...].astype(F32), axis=1, keepdims=True) + fgate_bias_ref[0]
     forget_log = jnp.minimum(fpre, 0.0) - jnp.log1p(jnp.exp(-jnp.abs(fpre)))
     carried = forget_log + column_of(log_scale_ref[...])
     new_max = jnp.maximum(carried, in_pre)
@@ -295,7 +335,7 @@
         column_of(
             jnp.sum(
                 jnp.where(
-                    routes_ref[...] == lax.rem(ep + off, groups), route_weights_ref[...], 0.0
+                    routes_ref[...] == partner(off), route_weights_ref[...], 0.0
                 ),
                 axis=0,
                 keepdims=True,
@@ -312,13 +352,13 @@
     ffn_in = (rf * rms_scale(rf) * ffn_gain_ref[...]).astype(BF16)
     for h in range(2):
         rows[h] = ffn_in[:, h * half : (h + 1) * half]
-    for off in range(groups - 1, 0, -1):
+    for off in range(1, groups):
         copy = pltpu.make_async_remote_copy(
             src_ref=rows.at[core],
             dst_ref=inbox.at[core, off // 2],
             send_sem=rows_send.at[off],
             recv_sem=rows_recv.at[core, off // 2],
-            device_id=(lax.rem(ep + off, groups), 2 * chip + off % 2),
+            device_id=(partner(off), 2 * chip + off % 2),
             device_id_type=MESH,
         )
         copy.start()
@@ -341,61 +381,62 @@
 
     for copy in pairs:
         copy.wait_recv()
-    for slot in range(1, slots):
-        for h in range(2):
-            arrived(inbox.at[h, slot], rows_recv.at[h, slot])
-    x = [inbox[h].reshape(slots * seqs, half) for h in range(2)]
-
-    def into(weights, block):
-        return sum(
-            jnp.dot(
-                x[h], weights[block, h * half : (h + 1) * half, :], preferred_element_type=F32
-            )
-            for h in range(2)
-        )
-
-    act = [
-        (jax.nn.silu(into(gate_v, block)) * into(up_v, block)).astype(BF16) for block in range(2)
-    ]
-    for q in range(lanes):
-        parts[q] = (
-            sum(
-                jnp.dot(
-                    act[block],
-                    down_v[block, :, q * quarter : (q + 1) * quarter],
-                    preferred_element_type=F32,
-                )
-                for block in range(2)
-            )
-            .astype(BF16)
-            .reshape(slots, seqs, quarter)
-        )
 
     def result(slot, toff):
+        group = partner(2 * slot) + core * (1 - 2 * lax.rem(ep, 2))
         return pltpu.make_async_remote_copy(
             src_ref=parts.at[lax.rem(tp + toff, lanes), slot],
             dst_ref=results.at[2 * slot + core, chip],
             send_sem=parts_send.at[slot, toff],
             recv_sem=parts_recv.at[2 * slot + core, chip],
-            device_id=(
-                lax.rem(ep + groups - 2 * slot - core, groups),
-                lax.rem(tp + toff, lanes),
-            ),
+            device_id=(group, lax.rem(tp + toff, lanes)),
             device_id_type=MESH,
         )
 
-    for slot in range(slots - 1, -1, -1):
-        for toff in range(lanes - 1, -1, -1):
-            if slot or toff:
-                result(slot, toff).start()
-
-    @pl.when(core == 1)
-    def _():
-        result(0, 0).start()
-
-    @pl.when(core == 0)
-    def _():
-        results[0, chip] = parts[tp, 0]
+    for first, count in ((slot, 1) for slot in range(slots)):
+        for slot in range(max(first, 1), first + count):
+            for h in range(2):
+                arrived(inbox.at[h, slot], rows_recv.at[h, slot])
+        x = [inbox[h, first : first + count].reshape(count * seqs, half) for h in range(2)]
+
+        def into(weights, block):
+            return sum(
+                jnp.dot(
+                    x[h], weights[block, h * half : (h + 1) * half, :], preferred_element_type=F32
+                )
+                for h in range(2)
+            )
+
+        act = [
+            (jax.nn.silu(into(gate_v, block)) * into(up_v, block)).astype(BF16)
+            for block in range(2)
+        ]
+        for q in range(lanes):
+            parts[q, first : first + count] = (
+                sum(
+                    jnp.dot(
+                        act[block],
+                        down_v[block, :, q * quarter : (q + 1) * quarter],
+                        preferred_element_type=F32,
+                    )
+                    for block in range(2)
+                )
+                .astype(BF16)
+                .reshape(count, seqs, quarter)
+            )
+        for slot in range(first, first + count):
+            for toff in range(lanes - 1, -1, -1):
+                if slot or toff:
+                    result(slot, toff).start()
+        if first == 0:
+
+            @pl.when(core == 1)
+            def _():
+                result(0, 0).start()
+
+            @pl.when(core == 0)
+            def _():
+                results[0, chip] = parts[tp, 0]
 
     routed = None
     for off in range(groups):
@@ -489,43 +530,46 @@
     seqs, width = tokens.shape
     local_experts, _, hidden = expert_gate.shape
     top = routes.shape[1]
-    if local_experts != 1 or log_scale.shape[1] != 1 or 2 * top < groups or groups % 2 or lanes % 2:
+    if local_experts != 1 or log_scale.shape[1] != 1 or 2 * top < groups or groups & (groups - 1) or groups < 4 or lanes % 2:
         return routed_device(*args)
     quarter = width // lanes
     key_dim, value_dim = memory.shape[2:]
     vmem = pl.BlockSpec(memory_space=pltpu.VMEM)
     hbm = pl.BlockSpec(memory_space=pl.ANY)
+    smem = pl.BlockSpec(memory_space=pltpu.SMEM)
     dma = pltpu.SemaphoreType.DMA
     pieces = 4 if seqs % 4 == 0 else 1
     operands = (
         (tokens, hbm),
         (memory, hbm),
-        (log_scale.T, vmem),
-        (mix_gain_in.reshape(1, -1), vmem),
+        (log_scale.T, hbm),
+        (mix_gain_in.reshape(1, -1), hbm),
         (w_query, hbm),
         (w_key, hbm),
         (w_value, hbm),
-        (w_igate.T, vmem),
-        (w_fgate.T, vmem),
-        (igate_bias.reshape(1, 1), vmem),
-        (fgate_bias.reshape(1, 1), vmem),
-        (head_gain.reshape(1, -1), vmem),
+        (w_igate.T, hbm),
+        (w_fgate.T, hbm),
+        (igate_bias, smem),
+        (fgate_bias, smem),
+        (head_gain.reshape(1, -1), hbm),
         (w_output, hbm),
-        (mix_gain_out.reshape(1, -1), vmem),
-        (ffn_gain_in.reshape(1, -1), vmem),
-        (routes.T, vmem),
-        (route_weights.T, vmem),
+        (mix_gain_out.reshape(1, -1), hbm),
+        (ffn_gain_in.reshape(1, -1), hbm),
+        (routes.T, hbm),
+        (route_weights.T, hbm),
         (expert_gate, hbm),
         (expert_up, hbm),
         (expert_down, hbm),
-        (ffn_gain_out.reshape(1, -1), vmem),
+        (ffn_gain_out.reshape(1, -1), hbm),
     )
     return pl.pallas_call(
         functools.partial(layer_kernel, groups, lanes),
-        out_shape=jax.ShapeDtypeStruct((seqs, quarter), BF16),
+        out_shape=pltpu.VMEM((seqs, quarter), BF16),
         in_specs=[spec for _, spec in operands],
         out_specs=vmem,
         scratch_shapes=[
+            *[pltpu.VMEM(operands[i][0].shape, operands[i][0].dtype) for i in (2, 3, 7, 8, 11, 13, 14, 15, 16, 20)],
+            dma((10,)),
             pltpu.VMEM((seqs, width), BF16),
             pltpu.VMEM((seqs, key_dim, value_dim), F32),
             pltpu.VMEM(w_query.shape, BF16),
@@ -559,7 +603,7 @@
         compiler_params=pltpu.CompilerParams(
             collective_id=0,
             has_side_effects=True,
-            vmem_limit_bytes=60 * 1024 * 1024,
+            vmem_limit_bytes=59 * 1024 * 1024,
         ),
         name="layer",
     )(*[array for array, _ in operands])

time: 28 us -> 26.3 us (0.939)
  Pallas kernels: 25.1 us -> 24.2 us
  local copies, waits for them, and re-layouts: 1.3 us -> 0.6 us
    pallas_call x1, Pallas kernels: 25.1 us -> 24.2 us  [per_device(): pl.pallas_call(functools.partial(layer_kernel, groups, lanes), out_shape=...]
    unnamed x1, local copies, waits for them, and re-layouts: 1.3 us -> 0.6 us
where the time goes in v3:
time: 26.3 us; the launch traced here: 26.1 us
  Pallas kernels  24.2 us (92%)
  between operations  1.3 us (5%)
  local copies, waits for them, and re-layouts  0.6 us (2%)
    pallas_call x1, Pallas kernels, per_device(): pl.pallas_call(functools.partial(layer_kernel, groups, lanes), out_shape=...  24.2 us
    unnamed x1, local copies, waits for them, and re-layouts  0.6 us

profile of v3, /device:TPU:0, one launch (start us, length us, event | category | flops | bytes accessed | tf_op | source)
XLA Modules:
  0.0 26.1 jit_solution(5715038395065990005)
XLA Ops:
  1.3 24.2 %layer.1 = bf16[16,256]{1,0:T(8,128)(2,1)S(1)} custom-call(bf16[16,1024]{1,0:T(8,128)(2,1)} %tokens_hbm.1, f32[16,1,128,256]{3,2,1,0:T(8,128)} %memory_hbm.1, f32[1,16]{1,0:T(1,128)} %bitcast.19, f32[1,1024]{1,0:T(1,128)} %bitcast.10, bf16[1024,128]{1,0:T(8,128)(2,1)} %w_query_hbm.1, bf16[1024,128]{1,0:T(8,128)(2,1)} %w_key_hbm.1, ...), custom_call_target="tpu_custom_call" | custom-call | tf_op jit(solution)/shard_map/layer/pallas_call | solution.py:565
  25.5 0.6 %copy.23 = bf16[16,256]{1,0:T(8,128)(2,1)} copy(bf16[16,256]{1,0:T(8,128)(2,1)S(1)} %layer.1) | data formatting | bytes 16384
